TPU v7x, 32 devices: a whole 2x2x4 slice. The times are simulated.
32 devices in a mesh: sp: 16 (over z, y, core), tp: 2 (over x).
Axes of the slice: x: 2, y: 2, z: 4, core: 2. Of those that a mesh axis runs over, the one named last changes fastest.
Arguments:
- queries: bfloat16 [8192, 1024], P('sp', 'tp'), may hold values from -40 to 40
- keys_values: bfloat16 [8192, 4, 128], P('sp', 'tp'), may hold values from -40 to 40
- doc_ids: int32 [8192], P('sp'), may hold values from 0 to 3, never falling along the last dimension, each value on 1 to 4096 neighbouring positions
- head_sink: float32 [16], P('tp'), may hold values from 3 to 7
- out_weight: bfloat16 [1024, 2048], replicated, may hold values from -0.1875 to 0.1875
- hidden_in: bfloat16 [8192, 2048], P(('sp', 'tp')), may hold values from -0.59765625 to 0.59765625
- norm_gain: float32 [2048], replicated, may hold values from 0.1 to 1.9
- expert_gate: bfloat16 [32, 2048, 1024], P(('sp', 'tp')), may hold values from -0.125 to 0.125
- expert_up: bfloat16 [32, 2048, 1024], P(('sp', 'tp')), may hold values from -0.125 to 0.125
- expert_down: bfloat16 [32, 1024, 2048], P(('sp', 'tp')), may hold values from -0.1875 to 0.1875
- routes: int32 [8192, 2], P(('sp', 'tp')), may hold values from 0 to 31, all different within a row; in each aligned block of 256 rows (0 to 255, 256 to 511, ...) at most 32 rows name the same one
- route_weight: float32 [8192, 2], P(('sp', 'tp')), may hold values from 0.1 to 1
Outputs:
- layer_out: bfloat16 [8192, 2048], P(('sp', 'tp'))
Inputs may be any that keep to these rules, and one draw needn't show every extreme that they name: `routes`: in the rows of one device (aligned blocks of 256 tokens in order) no expert is named more than 32 times; some expert is named exactly 32 times in some blocks.
All inputs are finite; a program needn't handle non-finite values.
Results may differ from a plain program's by a relative error of at most 0.02.
Values may be sent and summed in bfloat16 or wider, within the bound.
No kernel may reach another device: no remote copies, remote signals or barrier semaphores. Data moves between devices by JAX's collectives and lax.ppermute only.
A program may use at most 64 MiB of HBM per device.

v0:
```python
import jax
import jax.numpy as jnp
from jax import lax
from jax.sharding import PartitionSpec as P

HD = 64
WIN = 128


def with_halo(cells, sides, width):
    for axis, dim in sides:
        count = lax.axis_size(axis)
        ends = count - 1
        head = lax.slice_in_dim(cells, 0, width, axis=dim)
        tail = lax.slice_in_dim(cells, cells.shape[dim] - width, cells.shape[dim], axis=dim)
        cells = jnp.concatenate(
            [
                lax.ppermute(tail, axis, [(i, (i + 1) % count) for i in range(ends)]),
                cells,
                lax.ppermute(head, axis, [((i + 1) % count, i) for i in range(ends)]),
            ],
            axis=dim,
        )
    return cells


def expert_rows(arrived, gate_w, up_w, down_w):
    width = arrived.shape[-1]
    flat_rows = arrived.reshape(-1, width)
    gate = jnp.dot(flat_rows, gate_w, preferred_element_type=jnp.float32)
    upper = jnp.dot(flat_rows, up_w, preferred_element_type=jnp.float32)
    expert_hidden = (jax.nn.silu(gate) * upper).astype(jnp.bfloat16)
    result = jnp.dot(expert_hidden, down_w, preferred_element_type=jnp.float32).astype(jnp.bfloat16)
    return result.reshape(arrived.shape[:-1] + (result.shape[-1],))


def shards(
    queries,
    keys_values,
    doc_ids,
    head_sink,
    out_weight,
    hidden_in,
    norm_gain,
    expert_gate,
    expert_up,
    expert_down,
    routes,
    route_weight,
):
    tok_here = queries.shape[0]
    heads_here = head_sink.shape[0]
    kv_here = keys_values.shape[1]
    group = heads_here // kv_here
    head_dim = keys_values.shape[2] // 2
    kv_ext, docs_ext = (
        with_halo(keys_values, (("sp", 0),), WIN),
        with_halo(doc_ids, (("sp", 0),), WIN),
    )
    offset = lax.axis_index("sp") * tok_here
    seq_total = lax.axis_size("sp") * tok_here
    span_rows = min(512, tok_here)
    sink_logit = head_sink.reshape(kv_here, group)[:, :, None, None]

    def one_span(span_index):
        first_row = span_index * span_rows
        q_span = queries.reshape(span_rows, kv_here, group, head_dim)
        scores = jnp.einsum(
            "qhgd,khd->hgqk", q_span, kv_ext[..., :head_dim], preferred_element_type=jnp.float32
        ) * HD ** (-0.5)
        query_pos = offset + first_row + jnp.arange(span_rows, dtype=jnp.int32)
        key_pos = offset + first_row - WIN + jnp.arange(span_rows + 2 * WIN, dtype=jnp.int32)
        inside = (key_pos >= 0) & (key_pos < seq_total)
        allowed = (
            (jnp.abs(key_pos[None, :] - query_pos[:, None]) <= WIN)
            & inside[None, :]
            & (docs_ext[None, :] == doc_ids[:, None])
        )
        masked = jnp.where(allowed, scores, -1e30)
        row_max = jnp.maximum(masked.max(-1, keepdims=True), sink_logit)
        exp_scores = jnp.where(allowed, jnp.exp(masked - row_max), 0.0)
        total_mass = exp_scores.sum(-1, keepdims=True) + jnp.exp(sink_logit - row_max)
        weights = (exp_scores / total_mass).astype(jnp.bfloat16)
        outcome = jnp.einsum(
            "hgqk,khd->qhgd", weights, kv_ext[..., head_dim:], preferred_element_type=jnp.float32
        )
        return outcome.astype(jnp.bfloat16).reshape(span_rows, heads_here * head_dim)

    attended = lax.map(one_span, jnp.arange(tok_here // span_rows, dtype=jnp.int32)).reshape(
        tok_here, -1
    )
    gathered = lax.all_to_all(attended, "tp", split_axis=0, concat_axis=1, tiled=True)
    projected = jnp.dot(gathered, out_weight, preferred_element_type=jnp.float32)
    mid_wide = (hidden_in.astype(jnp.float32) + projected).astype(jnp.bfloat16).astype(jnp.float32)
    normed = (
        mid_wide
        * lax.rsqrt(jnp.mean(mid_wide * mid_wide, axis=-1, keepdims=True) + 1e-06)
        * norm_gain
    ).astype(jnp.bfloat16)
    local_rows = normed.shape[0]
    topk = routes.shape[1]
    width = normed.shape[1]
    sp_count = lax.axis_size("sp")
    tp_count = lax.axis_size("tp")
    expert_count = sp_count * tp_count
    capacity = 2 * local_rows * topk // expert_count
    flat_routes = routes.reshape(-1)
    one_hot = (flat_routes[:, None] == jnp.arange(expert_count, dtype=jnp.int32)[None, :]).astype(
        jnp.int32
    )
    slot_rank = (jnp.cumsum(one_hot, axis=0) * one_hot).sum(-1) - 1
    slot_index = flat_routes * capacity + slot_rank
    repeated = jnp.repeat(normed, topk, axis=0)
    buffer_rows = (
        jnp.zeros((expert_count * capacity, width), jnp.bfloat16).at[slot_index].set(repeated)
    )
    sent = buffer_rows.reshape(expert_count, capacity, width)
    finished = expert_rows(
        lax.all_to_all(sent, ("sp", "tp"), split_axis=0, concat_axis=0, tiled=True),
        expert_gate[0],
        expert_up[0],
        expert_down[0],
    )
    returned = lax.all_to_all(finished, ("sp", "tp"), split_axis=0, concat_axis=0, tiled=True)
    returned = returned.reshape(expert_count * capacity, width)
    picked = returned[slot_index].astype(jnp.float32).reshape(local_rows, topk, width)
    mixture = jnp.sum(picked * route_weight[..., None], axis=1)
    return (mid_wide + mixture).astype(jnp.bfloat16)


def solution(mesh):
    placed = (
        P("sp", "tp"),
        P("sp", "tp", None),
        P("sp"),
        P("tp"),
        P(),
        P(("sp", "tp"), None),
        P(),
        P(("sp", "tp"), None, None),
        P(("sp", "tp"), None, None),
        P(("sp", "tp"), None, None),
        P(("sp", "tp"), None),
        P(("sp", "tp"), None),
    )
    return jax.shard_map(
        shards, mesh=mesh, in_specs=placed, out_specs=P(("sp", "tp"), None), check_vma=False
    )
```

profile of v0, /device:TPU:0, one launch (start us, length us, event | category | flops | bytes accessed | tf_op | source)
XLA Modules:
  0.0 292.3 jit_solution(11387573325899256415)
XLA Ops:
  0.8 2.4 collective-permute-start.2
  3.2 1.3 collective-permute-start.3
  5.6 5.2 %collective-permute-start = (bf16[128,2,128]{0,2,1:T(8,128)(2,1)S(1)}, bf16[128,2,128]{0,2,1:T(8,128)(2,1)S(1)}, u32[]{:S(2)}, u32[]{:S(2)}) collective-permute-start(bf16[128,2,128]{0,2,1:T(8,128)(2,1)S(1)} %get-tuple-element.19), channel_id=1, source_target_pairs={{0,2},{2,4},{4,6},{6,8},{8,10},{10,12},{12,14},{14,16},{16,18},{18... | collective-permute-start | bytes 196616 | tf_op jit(solution)/shard_map/ppermute | solution.py:18
  10.8 1.3 collective-permute-start.1
  18.1 1.5 fusion.22
  19.8 2.1 fusion
  21.9 3.1 %fusion.1 = f32[2,4,512]{2,1,0:T(4,128)S(1)} fusion(f32[2,768,512,4]{2,1,3,0:T(8,128)S(1)} %get-tuple-element.32, f32[2,4,512]{2,1,0:T(4,128)S(1)} %broadcast_maximum_fusion, pred[512,768]{0,1:T(8,128)(4,1)S(1)} %fusion.22), kind=kLoop, calls=%fused_computation.6 | loop fusion | flops 15724544 | bytes 13008896 | tf_op jit(solution)/shard_map/while/body/eval_jaxpr/reduce_sum | solution.py:82
  25.1 3.9 %fusion.24 = bf16[512,2,4,64]{0,3,2,1:T(8,128)(2,1)S(1)} fusion(f32[2,768,512,4]{2,1,3,0:T(8,128)S(1)} %get-tuple-element.32, f32[2,4,512]{2,1,0:T(4,128)S(1)} %exponential_add_fusion, f32[2,4,512]{2,1,0:T(4,128)S(1)} %broadcast_maximum_fusion, pred[512,768]{0,1:T(8,128)(4,1)S(1)} %fusion.22, bf16[768,2,128]{0,2,1:T(8,128)(2,1)S(1)} %pad_maximum_fusion), kind=kOutput, calls=%fused_computation.32 | convolution fusion | flops 421789696 | bytes 13729792 | tf_op jit(solution)/shard_map/while/body/eval_jaxpr/hgqk,khd->qhgd/dot_general | solution.py:84
  30.0 3.7 %all-to-all-start = ((bf16[2,256,512]{1,2,0:T(8,128)(2,1)}), bf16[2,256,512]{1,2,0:T(8,128)(2,1)S(1)}, u32[]{:S(2)}, u32[]{:S(2)}) async-start(bf16[2,256,512]{1,2,0:T(8,128)(2,1)} %copy.24), calls=%async_computation | async-start | bytes 1048576 | tf_op jit(solution)/shard_map/all_to_all | solution.py:92
  34.0 7.5 %all-to-all-done = bf16[2,256,512]{1,2,0:T(8,128)(2,1)S(1)} async-done(((bf16[2,256,512]{1,2,0:T(8,128)(2,1)}), bf16[2,256,512]{1,2,0:T(8,128)(2,1)S(1)}, u32[]{:S(2)}, u32[]{:S(2)}) %all-to-all-start) | async-done | bytes 524320 | tf_op jit(solution)/shard_map/all_to_all | solution.py:92
  41.5 3.6 %fusion.15 = (f32[256]{0:T(256)S(1)}, bf16[256,2048]{1,0:T(8,128)(2,1)S(1)}) fusion(bf16[256,1024]{0,1:T(8,128)(2,1)S(1)} %bitcast.82, bf16[1024,2048]{1,0:T(8,128)(2,1)} %param.16, bf16[256,2048]{1,0:T(8,128)(2,1)S(1)} %copy-done.5), kind=kOutput, calls=%fused_computation.22 | convolution fusion | flops 1076887296 | bytes 6816768 | tf_op jit(solution)/shard_map/dot_general | solution.py:93
  45.5 1.3 broadcast_in_dim.49
  46.7 2.2 reshape.145
  49.0 7.2 %scatter_custom_fusion = bf16[1024,2048]{1,0:T(8,128)(2,1)} fusion(s32[512]{0:T(512)S(1)} %bitcast.83, bf16[512,2048]{1,0:T(8,128)(2,1)} %reshape.145, bf16[]{:T(256)} %constant.60.clone.1), kind=kCustom, calls=%fused_computation.26 | custom fusion | bytes 4194816 | tf_op jit(solution)/shard_map/scatter | solution.py:115
  56.2 101.2 %all_to_all.29 = bf16[32,32,2048]{2,1,0:T(8,128)(2,1)S(1)} all-to-all(bf16[32,32,2048]{2,1,0:T(8,128)(2,1)} %bitcast.77), channel_id=1, replica_groups=mesh['sp'=16,'tp'=2] {'sp','tp'}, dimensions={0} | all-to-all | bytes 8388608 | tf_op jit(solution)/shard_map/all_to_all | solution.py:119
  157.4 4.5 %fusion.5 = f32[1024,1024]{1,0:T(8,128)S(1)} fusion(bf16[1024,2048]{1,0:T(8,128)(2,1)S(1)} %bitcast.79, bf16[1,2048,1024]{2,1,0:T(8,128)(2,1)S(1)} %copy-done.2), kind=kOutput, calls=%fused_computation.10 | convolution fusion | flops 4294967296 | bytes 12582912 | tf_op jit(solution)/shard_map/dot_general | solution.py:31
  162.0 5.4 %multiply_convert_fusion = bf16[1024,1024]{1,0:T(8,128)(2,1)S(1)} fusion(f32[1024,1024]{1,0:T(8,128)S(1)} %fusion.5, bf16[1024,2048]{1,0:T(8,128)(2,1)S(1)} %bitcast.80, bf16[1,2048,1024]{2,1,0:T(8,128)(2,1)S(1)} %copy-done.3), kind=kOutput, calls=%fused_computation.15 | convolution fusion | flops 4301258752 | bytes 14680064 | tf_op jit(solution)/shard_map/dot_general | solution.py:30
  167.4 6.1 %fusion.9 = bf16[1024,2048]{1,0:T(8,128)(2,1)} fusion(bf16[1024,1024]{1,0:T(8,128)(2,1)S(1)} %multiply_convert_fusion, bf16[1,1024,2048]{2,1,0:T(8,128)(2,1)S(1)} %copy-done.4), kind=kOutput, calls=%fused_computation.16 | convolution fusion | flops 4297064448 | bytes 10485760 | tf_op jit(solution)/shard_map/dot_general | solution.py:33
  173.5 4.0 %all-to-all-start.2 = ((bf16[32,32,2048]{2,1,0:T(8,128)(2,1)}), bf16[32,32,2048]{2,1,0:T(8,128)(2,1)}, u32[]{:S(2)}, u32[]{:S(2)}) async-start(bf16[32,32,2048]{2,1,0:T(8,128)(2,1)} %bitcast.78), calls=%async_computation.2 | async-start | bytes 8388608 | tf_op jit(solution)/shard_map/all_to_all | solution.py:124
  177.7 93.3 %all-to-all-done.2 = bf16[32,32,2048]{2,1,0:T(8,128)(2,1)} async-done(((bf16[32,32,2048]{2,1,0:T(8,128)(2,1)}), bf16[32,32,2048]{2,1,0:T(8,128)(2,1)}, u32[]{:S(2)}, u32[]{:S(2)}) %all-to-all-start.2) | async-done | bytes 4194336 | tf_op jit(solution)/shard_map/all_to_all | solution.py:124
  271.0 7.1 %gather_fusion = bf16[512,2048]{1,0:T(8,128)(2,1)S(1)} fusion(bf16[1024,2048]{1,0:T(8,128)(2,1)} %bitcast.18, s32[1024]{0:T(1024)S(1)} %pad_clamp_fusion), kind=kCustom, calls=%fused_computation | custom fusion | bytes 4196352 | tf_op jit(solution)/shard_map/gather | solution.py:126
  278.1 4.0 %reshape.132 = f32[256,2,2048]{2,1,0:T(2,128)} reshape(bf16[512,2048]{1,0:T(8,128)(2,1)S(1)} %gather_fusion) | data formatting | bytes 6291456 | tf_op jit(solution)/shard_map/convert_element_type | solution.py:126
  282.1 8.9 %multiply_reduce_fusion = f32[256,2048]{1,0:T(8,128)S(1)} fusion(f32[256,2,2048]{2,1,0:T(2,128)} %reshape.132, f32[256,2]{1,0:T(8,128)S(1)} %copy.29), kind=kLoop, calls=%fused_computation.14 | loop fusion | flops 1572864 | bytes 6293504 | tf_op jit(solution)/shard_map/reduce_sum | solution.py:127
  291.0 1.3 fusion.18
  (48 shorter events, 9.9 us)
Async XLA Ops:
  0.8 16.7 %collective-permute-start.2 = (s32[128]{0:T(128)S(1)}, s32[128]{0:T(128)S(1)}, u32[]{:S(2)}, u32[]{:S(2)}) collective-permute-start(s32[128]{0:T(128)S(1)} %get-tuple-element.21), channel_id=1, source_target_pairs={{0,2},{2,4},{4,6},{6,8},{8,10},{10,12},{12,14},{14,16},{16,18},{18... | collective-permute-start | bytes 1544 | tf_op jit(solution)/shard_map/ppermute | solution.py:18
  3.2 14.3 %collective-permute-start.3 = (s32[128]{0:T(128)S(1)}, s32[128]{0:T(128)S(1)}, u32[]{:S(2)}, u32[]{:S(2)}) collective-permute-start(s32[128]{0:T(128)S(1)} %get-tuple-element.22), channel_id=1, source_target_pairs={{2,0},{4,2},{6,4},{8,6},{10,8},{12,10},{14,12},{16,14},{18,16},{20... | collective-permute-start | bytes 1544 | tf_op jit(solution)/shard_map/ppermute | solution.py:20
  5.6 14.1 %collective-permute-start = (bf16[128,2,128]{0,2,1:T(8,128)(2,1)S(1)}, bf16[128,2,128]{0,2,1:T(8,128)(2,1)S(1)}, u32[]{:S(2)}, u32[]{:S(2)}) collective-permute-start(bf16[128,2,128]{0,2,1:T(8,128)(2,1)S(1)} %get-tuple-element.19), channel_id=1, source_target_pairs={{0,2},{2,4},{4,6},{6,8},{8,10},{10,12},{12,14},{14,16},{16,18},{18... | collective-permute-start | bytes 196616 | tf_op jit(solution)/shard_map/ppermute | solution.py:18
  10.8 8.9 %collective-permute-start.1 = (bf16[128,2,128]{0,2,1:T(8,128)(2,1)S(1)}, bf16[128,2,128]{0,2,1:T(8,128)(2,1)S(1)}, u32[]{:S(2)}, u32[]{:S(2)}) collective-permute-start(bf16[128,2,128]{0,2,1:T(8,128)(2,1)S(1)} %get-tuple-element.20), channel_id=1, source_target_pairs={{2,0},{4,2},{6,4},{8,6},{10,8},{12,10},{14,12},{16,14},{18,16},{20... | collective-permute-start | bytes 196616 | tf_op jit(solution)/shard_map/ppermute | solution.py:20
  25.1 16.4 %copy-start.5 = (bf16[256,2048]{1,0:T(8,128)(2,1)S(1)}, bf16[256,2048]{1,0:T(8,128)(2,1)}, u32[]{:S(2)}) copy-start(bf16[256,2048]{1,0:T(8,128)(2,1)} %param.17) | copy-start | bytes 3145732
  30.0 11.5 %all-to-all-start = ((bf16[2,256,512]{1,2,0:T(8,128)(2,1)}), bf16[2,256,512]{1,2,0:T(8,128)(2,1)S(1)}, u32[]{:S(2)}, u32[]{:S(2)}) async-start(bf16[2,256,512]{1,2,0:T(8,128)(2,1)} %copy.24), calls=%async_computation | async-start | bytes 1048576 | tf_op jit(solution)/shard_map/all_to_all | solution.py:92
  34.0 11.1 %copy-start = (f32[2048]{0:T(1024)S(1)}, f32[2048]{0:T(1024)}, u32[]{:S(2)}) copy-start(f32[2048]{0:T(1024)} %param.18) | copy-start | bytes 24580
  56.2 101.2 %copy-start.2 = (bf16[1,2048,1024]{2,1,0:T(8,128)(2,1)S(1)}, bf16[1,2048,1024]{2,1,0:T(8,128)(2,1)}, u32[]{:S(2)}) copy-start(bf16[1,2048,1024]{2,1,0:T(8,128)(2,1)} %param.20) | copy-start | bytes 12582916
  157.4 4.5 %copy-start.3 = (bf16[1,2048,1024]{2,1,0:T(8,128)(2,1)S(1)}, bf16[1,2048,1024]{2,1,0:T(8,128)(2,1)}, u32[]{:S(2)}) copy-start(bf16[1,2048,1024]{2,1,0:T(8,128)(2,1)} %param.19) | copy-start | bytes 12582916
  162.0 5.4 %copy-start.4 = (bf16[1,1024,2048]{2,1,0:T(8,128)(2,1)S(1)}, bf16[1,1024,2048]{2,1,0:T(8,128)(2,1)}, u32[]{:S(2)}) copy-start(bf16[1,1024,2048]{2,1,0:T(8,128)(2,1)} %param.21) | copy-start | bytes 12582916
  173.5 4.0 %copy-start.1 = (f32[256,2]{0,1:T(2,128)S(1)}, f32[256,2]{0,1:T(2,128)}, u32[]{:S(2)}) copy-start(f32[256,2]{0,1:T(2,128)} %param.23) | copy-start | bytes 6148
  173.5 97.5 %all-to-all-start.2 = ((bf16[32,32,2048]{2,1,0:T(8,128)(2,1)}), bf16[32,32,2048]{2,1,0:T(8,128)(2,1)}, u32[]{:S(2)}, u32[]{:S(2)}) async-start(bf16[32,32,2048]{2,1,0:T(8,128)(2,1)} %bitcast.78), calls=%async_computation.2 | async-start | bytes 8388608 | tf_op jit(solution)/shard_map/all_to_all | solution.py:124
where the time goes:
time: 293 us; the launch traced here: 292 us
  waiting for transfers between devices  101 us (34%)
  blocking collectives  101 us (34%)
  local copies, waits for them, and re-layouts  28.5 us (10%)
  matrix products  25.7 us (9%)
  other arithmetic  18 us (6%)
  starting transfers between devices  17.8 us (6%)
    all_to_all x1, blocking collectives, shards(): lax.all_to_all(sent, ('sp', 'tp'), split_axis=0, concat_axis=0, tiled=True)  101 us
    all_to_all x1, waiting for transfers between devices, shards(): lax.all_to_all(finished, ('sp', 'tp'), split_axis=0, concat_axis=0, tiled...  93.3 us
    reduce_sum x1, other arithmetic, shards(): mixture = jnp.sum(picked * route_weight[..., None], axis=1)  8.89 us
    ppermute x2, starting transfers between devices, with_halo(): lax.ppermute(tail, axis, [(i, (i + 1) % count) for i in range(ends)])  7.54 us
    all_to_all x1, waiting for transfers between devices, shards(): lax.all_to_all(attended, 'tp', split_axis=0, concat_axis=1, tiled=True)  7.47 us
    scatter x1, local copies, waits for them, and re-layouts, shards(): jnp.zeros((expert_count * capacity, width), jnp.bfloat16).at[slot_index]  7.21 us
    gather x1, local copies, waits for them, and re-layouts, shards(): returned[slot_index].astype(jnp.float32).reshape(local_rows, topk, width)  7.13 us
    dot_general x1, matrix products, expert_rows(): jnp.dot(expert_hidden, down_w, preferred_element_type=jnp.float32)  6.15 us
  transfers between devices with their start and end apart: 6, of which 2 were waited for; matrix products, arithmetic and copies ran while one was open for 3% of the time, Pallas kernels for 0%

commit v1 on v0

v1 whole, which is shorter than its diff:
```python
import jax
import jax.numpy as jnp
from jax import lax
from jax.sharding import Mesh, PartitionSpec as P

HD = 64
WIN = 128
BF = jnp.bfloat16
F32 = jnp.float32
SP = ("half", "rest")
GROUP = ("rest", "tp")
ALL = ("half", "rest", "tp")
SWAP = [(0, 1), (1, 0)]


def with_halo(cells, width):
    count = lax.axis_size(SP)
    head = lax.slice_in_dim(cells, 0, width, axis=0)
    tail = lax.slice_in_dim(cells, cells.shape[0] - width, cells.shape[0], axis=0)
    return jnp.concatenate(
        [
            lax.ppermute(tail, SP, [(i, i + 1) for i in range(count - 1)]),
            cells,
            lax.ppermute(head, SP, [(i + 1, i) for i in range(count - 1)]),
        ],
        axis=0,
    )


def attention(queries, keys_values, doc_ids, head_sink):
    tok_here = queries.shape[0]
    heads_here = head_sink.shape[0]
    kv_here = keys_values.shape[1]
    group = heads_here // kv_here
    head_dim = keys_values.shape[2] // 2
    kv_ext, docs_ext = with_halo(keys_values, WIN), with_halo(doc_ids, WIN)
    offset = lax.axis_index(SP) * tok_here
    seq_total = lax.axis_size(SP) * tok_here
    sink_logit = head_sink.reshape(kv_here, group)[:, :, None, None]
    q_span = queries.reshape(tok_here, kv_here, group, head_dim)
    scores = jnp.einsum(
        "qhgd,khd->hgqk", q_span, kv_ext[..., :head_dim], preferred_element_type=F32
    ) * HD ** (-0.5)
    query_pos = offset + jnp.arange(tok_here, dtype=jnp.int32)
    key_pos = offset - WIN + jnp.arange(tok_here + 2 * WIN, dtype=jnp.int32)
    inside = (key_pos >= 0) & (key_pos < seq_total)
    allowed = (
        (jnp.abs(key_pos[None, :] - query_pos[:, None]) <= WIN)
        & inside[None, :]
        & (docs_ext[None, :] == doc_ids[:, None])
    )
    masked = jnp.where(allowed, scores, -1e30)
    row_max = jnp.maximum(masked.max(-1, keepdims=True), sink_logit)
    exp_scores = jnp.where(allowed, jnp.exp(masked - row_max), 0.0)
    total_mass = exp_scores.sum(-1, keepdims=True) + jnp.exp(sink_logit - row_max)
    weights = (exp_scores / total_mass).astype(BF)
    outcome = jnp.einsum(
        "hgqk,khd->qhgd", weights, kv_ext[..., head_dim:], preferred_element_type=F32
    )
    return outcome.astype(BF).reshape(tok_here, heads_here * head_dim)


def slot_maps(routes, route_weight, first, experts, capacity):
    tokens = routes.shape[0]
    names = first + jnp.arange(experts, dtype=jnp.int32)
    hits = routes.T[None, :, :] == names[:, None, None]
    named = hits.any(1)
    weight = jnp.where(hits, route_weight.T[None], 0.0).sum(1)
    at = jnp.arange(tokens, dtype=jnp.int32)
    earlier = (at[:, None] < at[None, :]).astype(BF)
    rank = jnp.dot(named.astype(BF), earlier, preferred_element_type=F32)
    rank = jnp.where(named, rank, -1.0).astype(jnp.int32)
    slots = jnp.arange(capacity, dtype=jnp.int32)
    pick = rank[:, None, :] == slots[None, :, None]
    mix = jnp.where(pick, weight[:, None, :], 0.0)
    shape = (experts * capacity, tokens)
    return pick.astype(BF).reshape(shape), mix.reshape(shape)


def exchange(rows, experts):
    cut = rows.reshape(experts, -1, rows.shape[-1])
    return lax.all_to_all(cut, GROUP, split_axis=0, concat_axis=0, tiled=True).reshape(rows.shape)


def dispatch(pick, normed, experts):
    rows = jnp.dot(pick, normed, preferred_element_type=F32).astype(BF)
    return exchange(rows, experts)


def expert_rows(rows, gate_w, up_w, down_w):
    gate = jnp.dot(rows, gate_w, preferred_element_type=F32)
    upper = jnp.dot(rows, up_w, preferred_element_type=F32)
    hidden = (jax.nn.silu(gate) * upper).astype(BF)
    return jnp.dot(hidden, down_w, preferred_element_type=F32).astype(BF)


def combine(mix, rows):
    high = mix.astype(BF)
    low = (mix - high.astype(F32)).astype(BF)

    def part(m):
        return lax.dot_general(m, rows, (((0,), (0,)), ((), ())), preferred_element_type=F32)

    return part(high) + part(low)


def shards(
    queries,
    keys_values,
    doc_ids,
    head_sink,
    out_weight,
    hidden_in,
    norm_gain,
    expert_gate,
    expert_up,
    expert_down,
    routes,
    route_weight,
):
    attended = attention(queries, keys_values, doc_ids, head_sink)
    gathered = lax.all_to_all(attended, "tp", split_axis=0, concat_axis=1, tiled=True)
    projected = jnp.dot(gathered, out_weight, preferred_element_type=F32)
    mid = (hidden_in.astype(F32) + projected).astype(BF)
    mid_wide = mid.astype(F32)
    normed = (
        mid_wide
        * lax.rsqrt(jnp.mean(mid_wide * mid_wide, axis=-1, keepdims=True) + 1e-06)
        * norm_gain
    ).astype(BF)

    experts = lax.axis_size(GROUP)
    capacity = 2 * routes.shape[0] * routes.shape[1] // (2 * experts)
    first = lax.axis_index("half") * experts
    routes_far = lax.ppermute(routes, "half", SWAP)
    weight_far = lax.ppermute(route_weight, "half", SWAP)
    normed_far = lax.ppermute(normed, "half", SWAP)
    pick_near, mix_near = slot_maps(routes, route_weight, first, experts, capacity)
    pick_far, mix_far = slot_maps(routes_far, weight_far, first, experts, capacity)
    weights = (expert_gate[0], expert_up[0], expert_down[0])
    rows_near = expert_rows(dispatch(pick_near, normed, experts), *weights)
    rows_far = expert_rows(dispatch(pick_far, normed_far, experts), *weights)
    share_far = combine(mix_far, exchange(rows_far, experts)).astype(BF)
    share_back = lax.ppermute(share_far, "half", SWAP)
    share_near = combine(mix_near, exchange(rows_near, experts))
    return (mid.astype(F32) + share_near + share_back.astype(F32)).astype(BF)


def solution(mesh):
    sp, tp = mesh.shape["sp"], mesh.shape["tp"]
    halves = Mesh(mesh.devices.reshape(2, sp // 2, tp), ALL)
    placed = (
        P(SP, "tp"),
        P(SP, "tp", None),
        P(SP),
        P("tp"),
        P(),
        P(ALL, None),
        P(),
        P(ALL, None, None),
        P(ALL, None, None),
        P(ALL, None, None),
        P(ALL, None),
        P(ALL, None),
    )
    return jax.shard_map(
        shards, mesh=halves, in_specs=placed, out_specs=P(ALL, None), check_vma=False
    )
```

time: 293 us -> 280 us (0.956)
  blocking collectives: 101 us -> 10.8 us
  waiting for transfers between devices: 101 us -> 160 us
  matrix products: 25.7 us -> 53.9 us
  starting transfers between devices: 17.8 us -> 41.1 us
  local copies, waits for them, and re-layouts: 28.5 us -> 6.57 us
  other arithmetic: 18 us -> 6.2 us
    ppermute x4 -> x8, waiting for transfers between devices: 0.01 us -> 113 us  [the longest x1 44.9 us: shards(): share_back = lax.ppermute(share_far, 'half', SWAP)]
    all_to_all x1, blocking collectives: 101 us -> 10.8 us  [shards(): lax.all_to_all(attended, 'tp', split_axis=0, concat_axis=1, tiled=True)]
    all_to_all x2 -> x4, waiting for transfers between devices: 101 us -> 47.2 us  [exchange(): lax.all_to_all(cut, GROUP, split_axis=0, concat_axis=0, tiled=True)]
    dot_general x6 -> x15, matrix products: 25.7 us -> 53.9 us  [the longest x2 20.5 us: expert_rows(): return jnp.dot(hidden, down_w, preferred_element_type=F32).astype(BF)]
    all_to_all x2 -> x4, starting transfers between devices: 7.7 us -> 20.8 us  [exchange(): lax.all_to_all(cut, GROUP, split_axis=0, concat_axis=0, tiled=True)]
    ppermute x4 -> x8, starting transfers between devices: 10.1 us -> 20.2 us  [the longest x2 7.54 us: with_halo(): lax.ppermute(tail, SP, [(i, i + 1) for i in range(count - 1)])]
    reduce_sum x3 -> x2, other arithmetic: 12.1 us -> 3.13 us  [the longest x1 3.06 us: attention(): exp_scores.sum(-1, keepdims=True) + jnp.exp(sink_logit - row_max)]
    scatter x1 -> x0, local copies, waits for them, and re-layouts: 7.21 us -> none  [shards(): jnp.zeros((expert_count * capacity, width), jnp.bfloat16).at[slot_index]]
  transfers between devices with their start and end apart: 6 -> 12, of which waited for: 2 -> 6; matrix products, arithmetic and copies ran while one was open for 3% -> 16% of each run, Pallas kernels for 0% -> 0%
where the time goes in v1:
time: 280 us; the launch traced here: 279 us
  waiting for transfers between devices  160 us (57%)
  matrix products  53.9 us (19%)
  starting transfers between devices  41.1 us (15%)
  blocking collectives  10.8 us (4%)
  local copies, waits for them, and re-layouts  6.57 us (2%)
  other arithmetic  6.2 us (2%)
    all_to_all x4, waiting for transfers between devices, exchange(): lax.all_to_all(cut, GROUP, split_axis=0, concat_axis=0, tiled=True)  47.2 us
    ppermute x1, waiting for transfers between devices, shards(): share_back = lax.ppermute(share_far, 'half', SWAP)  44.9 us
    ppermute x1, waiting for transfers between devices, shards(): routes_far = lax.ppermute(routes, 'half', SWAP)  43.6 us
    ppermute x1, waiting for transfers between devices, shards(): weight_far = lax.ppermute(route_weight, 'half', SWAP)  24.6 us
    all_to_all x4, starting transfers between devices, exchange(): lax.all_to_all(cut, GROUP, split_axis=0, concat_axis=0, tiled=True)  20.8 us
    dot_general x2, matrix products, expert_rows(): return jnp.dot(hidden, down_w, preferred_element_type=F32).astype(BF)  20.5 us
    dot_general x2, matrix products, expert_rows(): gate = jnp.dot(rows, gate_w, preferred_element_type=F32)  12.4 us
    all_to_all x1, blocking collectives, shards(): lax.all_to_all(attended, 'tp', split_axis=0, concat_axis=1, tiled=True)  10.8 us
  transfers between devices with their start and end apart: 12, of which 6 were waited for; matrix products, arithmetic and copies ran while one was open for 16% of the time, Pallas kernels for 0%

profile of v1, /device:TPU:0, one launch (start us, length us, event | category | flops | bytes accessed | tf_op | source)
XLA Modules:
  0.0 279.1 jit_solution(8157586746678905649)
XLA Ops:
  0.8 2.4 collective-permute-start.2
  5.6 5.2 %collective-permute-start = (bf16[128,2,128]{0,2,1:T(8,128)(2,1)S(1)}, bf16[128,2,128]{0,2,1:T(8,128)(2,1)S(1)}, u32[]{:S(2)}, u32[]{:S(2)}) collective-permute-start(bf16[128,2,128]{0,2,1:T(8,128)(2,1)S(1)} %get-tuple-element.9), channel_id=1, source_target_pairs={{0,2},{2,4},{4,6},{6,8},{8,10},{10,12},{12,14},{14,16},{16,18},{18... | collective-permute-start | bytes 196616 | tf_op jit(solution)/shard_map/ppermute | solution.py:22
  16.4 2.1 fusion
  18.6 3.1 %fusion.1 = f32[2,4,512]{2,1,0:T(4,128)S(1)} fusion(f32[2,768,512,4]{2,1,3,0:T(8,128)S(1)} %get-tuple-element.16, f32[2,4,512]{2,1,0:T(4,128)S(1)} %broadcast_maximum_fusion, pred[512,768]{0,1:T(8,128)(4,1)S(1)} %fusion.33), kind=kLoop, calls=%fused_computation.4 | loop fusion | flops 15724544 | bytes 13008896 | tf_op jit(solution)/shard_map/reduce_sum | solution.py:55
  21.8 3.9 %fusion.35 = bf16[512,2,4,64]{0,3,2,1:T(8,128)(2,1)S(1)} fusion(f32[2,768,512,4]{2,1,3,0:T(8,128)S(1)} %get-tuple-element.16, f32[2,4,512]{2,1,0:T(4,128)S(1)} %exponential_add_fusion, f32[2,4,512]{2,1,0:T(4,128)S(1)} %broadcast_maximum_fusion, pred[512,768]{0,1:T(8,128)(4,1)S(1)} %fusion.33, bf16[768,2,128]{0,2,1:T(8,128)(2,1)S(1)} %pad_maximum_fusion), kind=kOutput, calls=%fused_computation.44 | convolution fusion | flops 421789696 | bytes 13729792 | tf_op jit(solution)/shard_map/hgqk,khd->qhgd/dot_general | solution.py:57
  25.9 10.8 %all_to_all.39 = bf16[2,256,512]{1,2,0:T(8,128)(2,1)S(1)} all-to-all(bf16[2,256,512]{1,2,0:T(8,128)(2,1)S(1)} %copy.29), channel_id=1, replica_groups=mesh['half'=2,'rest'=8,'tp'=2] {'tp'}, dimensions={0} | all-to-all | bytes 1048576 | tf_op jit(solution)/shard_map/all_to_all | solution.py:122
  36.8 3.6 %fusion.25 = (f32[256]{0:T(256)S(1)}, bf16[256,2048]{1,0:T(8,128)(2,1)S(1)}) fusion(bf16[256,1024]{0,1:T(8,128)(2,1)S(1)} %bitcast.118, bf16[1024,2048]{1,0:T(8,128)(2,1)} %param.16, bf16[256,2048]{1,0:T(8,128)(2,1)S(1)} %copy-done.7), kind=kOutput, calls=%fused_computation.34 | convolution fusion | flops 1076887296 | bytes 6816768 | tf_op jit(solution)/shard_map/dot_general | solution.py:123
  41.8 5.4 %collective-permute-start.6 = (bf16[256,2048]{1,0:T(8,128)(2,1)S(1)}, bf16[256,2048]{1,0:T(8,128)(2,1)S(1)}, u32[]{:S(2)}, u32[]{:S(2)}) collective-permute-start(bf16[256,2048]{1,0:T(8,128)(2,1)S(1)} %fusion.27), channel_id=1, source_target_pairs={{0,16},{16,0},{1,17},{17,1},{2,18},{18,2},{3,19},{19,3},{4,20},{20... | collective-permute-start | bytes 3145736 | tf_op jit(solution)/shard_map/ppermute | solution.py:137
  47.3 43.6 %collective-permute-done.4 = s32[256,2]{0,1:T(2,128)S(1)} collective-permute-done((s32[256,2]{0,1:T(2,128)S(1)}, s32[256,2]{0,1:T(2,128)S(1)}, u32[]{:S(2)}, u32[]{:S(2)}) %collective-permute-start.4) | collective-permute-done | bytes 2080 | tf_op jit(solution)/shard_map/ppermute | solution.py:135
  93.6 6.0 %all-to-all-start.3 = ((bf16[16,32,2048]{2,1,0:T(8,128)(2,1)}), bf16[16,32,2048]{2,1,0:T(8,128)(2,1)S(1)}, u32[]{:S(2)}, u32[]{:S(2)}) async-start(bf16[16,32,2048]{2,1,0:T(8,128)(2,1)} %bitcast.23), calls=%async_computation.3 | async-start | bytes 4194304 | tf_op jit(solution)/shard_map/all_to_all | solution.py:82
  101.7 25.0 %all-to-all-done.3 = bf16[16,32,2048]{2,1,0:T(8,128)(2,1)S(1)} async-done(((bf16[16,32,2048]{2,1,0:T(8,128)(2,1)}), bf16[16,32,2048]{2,1,0:T(8,128)(2,1)S(1)}, u32[]{:S(2)}, u32[]{:S(2)}) %all-to-all-start.3) | async-done | bytes 2097184 | tf_op jit(solution)/shard_map/all_to_all | solution.py:82
  126.7 5.3 %all-to-all-start.1 = ((bf16[16,32,2048]{2,1,0:T(8,128)(2,1)}), bf16[16,32,2048]{2,1,0:T(8,128)(2,1)}, u32[]{:S(2)}, u32[]{:S(2)}) async-start(bf16[16,32,2048]{2,1,0:T(8,128)(2,1)} %bitcast.12), calls=%async_computation.1 | async-start | bytes 4194304 | tf_op jit(solution)/shard_map/all_to_all | solution.py:82
  132.0 5.9 %fusion.11 = f32[512,1024]{1,0:T(8,128)} fusion(bf16[512,2048]{1,0:T(8,128)(2,1)S(1)} %bitcast.114, bf16[1,2048,1024]{2,1,0:T(8,128)(2,1)} %param.19), kind=kOutput, calls=%fused_computation.14 | convolution fusion | flops 2147483648 | bytes 8388608 | tf_op jit(solution)/shard_map/dot_general | solution.py:91
  137.9 10.0 %fusion.18 = bf16[512,2048]{1,0:T(8,128)(2,1)} fusion(bf16[1,1024,2048]{2,1,0:T(8,128)(2,1)} %param.21, f32[512,1024]{1,0:T(8,128)} %fusion.11, bf16[512,2048]{1,0:T(8,128)(2,1)S(1)} %bitcast.115, bf16[1,2048,1024]{2,1,0:T(8,128)(2,1)} %param.20), kind=kOutput, calls=%fused_computation.22 | convolution fusion | flops 4299161600 | bytes 14680064 | tf_op jit(solution)/shard_map/dot_general | solution.py:94
  147.8 12.2 %all-to-all-done.1 = bf16[16,32,2048]{2,1,0:T(8,128)(2,1)} async-done(((bf16[16,32,2048]{2,1,0:T(8,128)(2,1)}), bf16[16,32,2048]{2,1,0:T(8,128)(2,1)}, u32[]{:S(2)}, u32[]{:S(2)}) %all-to-all-start.1) | async-done | bytes 2097184 | tf_op jit(solution)/shard_map/all_to_all | solution.py:82
  160.0 4.3 %all-to-all-start.4 = ((bf16[16,32,2048]{2,1,0:T(8,128)(2,1)}), bf16[16,32,2048]{2,1,0:T(8,128)(2,1)S(1)}, u32[]{:S(2)}, u32[]{:S(2)}) async-start(bf16[16,32,2048]{2,1,0:T(8,128)(2,1)} %bitcast.116), calls=%async_computation.4 | async-start | bytes 4194304 | tf_op jit(solution)/shard_map/all_to_all | solution.py:82
  164.3 6.5 %fusion.13 = f32[512,1024]{1,0:T(8,128)} fusion(bf16[512,2048]{1,0:T(8,128)(2,1)} %bitcast.13, bf16[1,2048,1024]{2,1,0:T(8,128)(2,1)} %param.19), kind=kOutput, calls=%fused_computation.16 | convolution fusion | flops 2147483648 | bytes 8388608 | tf_op jit(solution)/shard_map/dot_general | solution.py:91
  170.8 10.6 %fusion.15 = bf16[512,2048]{1,0:T(8,128)(2,1)} fusion(bf16[1,1024,2048]{2,1,0:T(8,128)(2,1)} %param.21, f32[512,1024]{1,0:T(8,128)} %fusion.13, bf16[512,2048]{1,0:T(8,128)(2,1)} %bitcast.13, bf16[1,2048,1024]{2,1,0:T(8,128)(2,1)} %param.20), kind=kOutput, calls=%fused_computation.21 | convolution fusion | flops 4299161600 | bytes 14680064 | tf_op jit(solution)/shard_map/dot_general | solution.py:94
  181.4 10.0 %all-to-all-done.4 = bf16[16,32,2048]{2,1,0:T(8,128)(2,1)S(1)} async-done(((bf16[16,32,2048]{2,1,0:T(8,128)(2,1)}), bf16[16,32,2048]{2,1,0:T(8,128)(2,1)S(1)}, u32[]{:S(2)}, u32[]{:S(2)}) %all-to-all-start.4) | async-done | bytes 2097184 | tf_op jit(solution)/shard_map/all_to_all | solution.py:82
  192.8 5.2 %all-to-all-start.2 = ((bf16[16,32,2048]{2,1,0:T(8,128)(2,1)}), bf16[16,32,2048]{2,1,0:T(8,128)(2,1)S(1)}, u32[]{:S(2)}, u32[]{:S(2)}) async-start(bf16[16,32,2048]{2,1,0:T(8,128)(2,1)} %bitcast.113), calls=%async_computation.2 | async-start | bytes 4194304 | tf_op jit(solution)/shard_map/all_to_all | solution.py:82
  199.3 24.6 %collective-permute-done.5 = f32[256,2]{0,1:T(2,128)S(1)} collective-permute-done((f32[256,2]{0,1:T(2,128)S(1)}, f32[256,2]{0,1:T(2,128)S(1)}, u32[]{:S(2)}, u32[]{:S(2)}) %collective-permute-start.5) | collective-permute-done | bytes 2080 | tf_op jit(solution)/shard_map/ppermute | solution.py:136
  224.1 2.5 convolution_bitcast_fusion
  228.3 3.3 %collective-permute-start.7 = (bf16[256,2048]{1,0:T(8,128)(2,1)}, bf16[256,2048]{1,0:T(8,128)(2,1)S(1)}, u32[]{:S(2)}, u32[]{:S(2)}) collective-permute-start(bf16[256,2048]{1,0:T(8,128)(2,1)} %fusion.23), channel_id=1, source_target_pairs={{0,16},{16,0},{1,17},{17,1},{2,18},{18,2},{3,19},{19,3},{4,20},{20... | collective-permute-start | bytes 3145736 | tf_op jit(solution)/shard_map/ppermute | solution.py:144
  232.3 44.9 %collective-permute-done.7 = bf16[256,2048]{1,0:T(8,128)(2,1)S(1)} collective-permute-done((bf16[256,2048]{1,0:T(8,128)(2,1)}, bf16[256,2048]{1,0:T(8,128)(2,1)S(1)}, u32[]{:S(2)}, u32[]{:S(2)}) %collective-permute-start.7) | collective-permute-done | bytes 1048608 | tf_op jit(solution)/shard_map/ppermute | solution.py:144
  (56 shorter events, 22.6 us)
Async XLA Ops:
  0.8 13.4 %collective-permute-start.2 = (s32[128]{0:T(128)S(1)}, s32[128]{0:T(128)S(1)}, u32[]{:S(2)}, u32[]{:S(2)}) collective-permute-start(s32[128]{0:T(128)S(1)} %get-tuple-element.13), channel_id=1, source_target_pairs={{0,2},{2,4},{4,6},{6,8},{8,10},{10,12},{12,14},{14,16},{16,18},{18... | collective-permute-start | bytes 1544 | tf_op jit(solution)/shard_map/ppermute | solution.py:22
  3.2 11.0 %collective-permute-start.3 = (s32[128]{0:T(128)S(1)}, s32[128]{0:T(128)S(1)}, u32[]{:S(2)}, u32[]{:S(2)}) collective-permute-start(s32[128]{0:T(128)S(1)} %get-tuple-element.14), channel_id=1, source_target_pairs={{2,0},{4,2},{6,4},{8,6},{10,8},{12,10},{14,12},{16,14},{18,16},{20... | collective-permute-start | bytes 1544 | tf_op jit(solution)/shard_map/ppermute | solution.py:24
  5.6 10.8 %collective-permute-start = (bf16[128,2,128]{0,2,1:T(8,128)(2,1)S(1)}, bf16[128,2,128]{0,2,1:T(8,128)(2,1)S(1)}, u32[]{:S(2)}, u32[]{:S(2)}) collective-permute-start(bf16[128,2,128]{0,2,1:T(8,128)(2,1)S(1)} %get-tuple-element.9), channel_id=1, source_target_pairs={{0,2},{2,4},{4,6},{6,8},{8,10},{10,12},{12,14},{14,16},{16,18},{18... | collective-permute-start | bytes 196616 | tf_op jit(solution)/shard_map/ppermute | solution.py:22
  10.8 5.6 %collective-permute-start.1 = (bf16[128,2,128]{0,2,1:T(8,128)(2,1)S(1)}, bf16[128,2,128]{0,2,1:T(8,128)(2,1)S(1)}, u32[]{:S(2)}, u32[]{:S(2)}) collective-permute-start(bf16[128,2,128]{0,2,1:T(8,128)(2,1)S(1)} %get-tuple-element.10), channel_id=1, source_target_pairs={{2,0},{4,2},{6,4},{8,6},{10,8},{12,10},{14,12},{16,14},{18,16},{20... | collective-permute-start | bytes 196616 | tf_op jit(solution)/shard_map/ppermute | solution.py:24
  25.7 11.1 %copy-start.7 = (bf16[256,2048]{1,0:T(8,128)(2,1)S(1)}, bf16[256,2048]{1,0:T(8,128)(2,1)}, u32[]{:S(2)}) copy-start(bf16[256,2048]{1,0:T(8,128)(2,1)} %param.17) | copy-start | bytes 3145732
  36.8 4.7 %copy-start.4 = (f32[2048]{0:T(1024)S(1)}, f32[2048]{0:T(1024)}, u32[]{:S(2)}) copy-start(f32[2048]{0:T(1024)} %param.18) | copy-start | bytes 24580
  40.4 1.1 copy-start.2
  40.4 6.7 %copy-start.5 = (s32[256,2]{0,1:T(2,128)S(1)}, s32[256,2]{0,1:T(2,128)}, u32[]{:S(2)}) copy-start(s32[256,2]{0,1:T(2,128)} %param.22) | copy-start | bytes 6148
  41.8 49.7 %collective-permute-start.6 = (bf16[256,2048]{1,0:T(8,128)(2,1)S(1)}, bf16[256,2048]{1,0:T(8,128)(2,1)S(1)}, u32[]{:S(2)}, u32[]{:S(2)}) collective-permute-start(bf16[256,2048]{1,0:T(8,128)(2,1)S(1)} %fusion.27), channel_id=1, source_target_pairs={{0,16},{16,0},{1,17},{17,1},{2,18},{18,2},{3,19},{19,3},{4,20},{20... | collective-permute-start | bytes 3145736 | tf_op jit(solution)/shard_map/ppermute | solution.py:137
  47.1 43.7 %collective-permute-start.4 = (s32[256,2]{0,1:T(2,128)S(1)}, s32[256,2]{0,1:T(2,128)S(1)}, u32[]{:S(2)}, u32[]{:S(2)}) collective-permute-start(s32[256,2]{0,1:T(2,128)S(1)} %copy-done.5), channel_id=1, source_target_pairs={{0,16},{16,0},{1,17},{17,1},{2,18},{18,2},{3,19},{19,3},{4,20},{20... | collective-permute-start | bytes 6152 | tf_op jit(solution)/shard_map/ppermute | solution.py:135
  93.6 33.1 %all-to-all-start.3 = ((bf16[16,32,2048]{2,1,0:T(8,128)(2,1)}), bf16[16,32,2048]{2,1,0:T(8,128)(2,1)S(1)}, u32[]{:S(2)}, u32[]{:S(2)}) async-start(bf16[16,32,2048]{2,1,0:T(8,128)(2,1)} %bitcast.23), calls=%async_computation.3 | async-start | bytes 4194304 | tf_op jit(solution)/shard_map/all_to_all | solution.py:82
  126.7 33.4 %all-to-all-start.1 = ((bf16[16,32,2048]{2,1,0:T(8,128)(2,1)}), bf16[16,32,2048]{2,1,0:T(8,128)(2,1)}, u32[]{:S(2)}, u32[]{:S(2)}) async-start(bf16[16,32,2048]{2,1,0:T(8,128)(2,1)} %bitcast.12), calls=%async_computation.1 | async-start | bytes 4194304 | tf_op jit(solution)/shard_map/all_to_all | solution.py:82
  160.0 31.4 %all-to-all-start.4 = ((bf16[16,32,2048]{2,1,0:T(8,128)(2,1)}), bf16[16,32,2048]{2,1,0:T(8,128)(2,1)S(1)}, u32[]{:S(2)}, u32[]{:S(2)}) async-start(bf16[16,32,2048]{2,1,0:T(8,128)(2,1)} %bitcast.116), calls=%async_computation.4 | async-start | bytes 4194304 | tf_op jit(solution)/shard_map/all_to_all | solution.py:82
  191.4 1.3 copy-start
  191.4 6.5 %copy-start.6 = (f32[256,2]{0,1:T(2,128)S(1)}, f32[256,2]{0,1:T(2,128)}, u32[]{:S(2)}) copy-start(f32[256,2]{0,1:T(2,128)} %param.23) | copy-start | bytes 6148
  192.8 38.8 %all-to-all-start.2 = ((bf16[16,32,2048]{2,1,0:T(8,128)(2,1)}), bf16[16,32,2048]{2,1,0:T(8,128)(2,1)S(1)}, u32[]{:S(2)}, u32[]{:S(2)}) async-start(bf16[16,32,2048]{2,1,0:T(8,128)(2,1)} %bitcast.113), calls=%async_computation.2 | async-start | bytes 4194304 | tf_op jit(solution)/shard_map/all_to_all | solution.py:82
  198.0 26.0 %collective-permute-start.5 = (f32[256,2]{0,1:T(2,128)S(1)}, f32[256,2]{0,1:T(2,128)S(1)}, u32[]{:S(2)}, u32[]{:S(2)}) collective-permute-start(f32[256,2]{0,1:T(2,128)S(1)} %copy-done.6), channel_id=1, source_target_pairs={{0,16},{16,0},{1,17},{17,1},{2,18},{18,2},{3,19},{19,3},{4,20},{20... | collective-permute-start | bytes 6152 | tf_op jit(solution)/shard_map/ppermute | solution.py:136
  224.1 2.5 copy-start.1
  228.3 48.9 %collective-permute-start.7 = (bf16[256,2048]{1,0:T(8,128)(2,1)}, bf16[256,2048]{1,0:T(8,128)(2,1)S(1)}, u32[]{:S(2)}, u32[]{:S(2)}) collective-permute-start(bf16[256,2048]{1,0:T(8,128)(2,1)} %fusion.23), channel_id=1, source_target_pairs={{0,16},{16,0},{1,17},{17,1},{2,18},{18,2},{3,19},{19,3},{4,20},{20... | collective-permute-start | bytes 3145736 | tf_op jit(solution)/shard_map/ppermute | solution.py:144
  231.6 45.6 %copy-start.3 = (bf16[256,2048]{1,0:T(8,128)(2,1)S(1)}, bf16[256,2048]{1,0:T(8,128)(2,1)}, u32[]{:S(2)}) copy-start(bf16[256,2048]{1,0:T(8,128)(2,1)} %copy-done.2) | copy-start | bytes 3145732
